TPU v7x, 256 devices: a whole 4x4x8 slice. The times are simulated.
256 devices in a mesh: sp: 64 (over z, y, core), tp: 4 (over x).
Axes of the slice: x: 4, y: 4, z: 8, core: 2. Of those that a mesh axis runs over, the one named last changes fastest.
Arguments:
- tokens: bfloat16 [24576, 2048], P(('sp', 'tp')), may hold values from -60 to 60
- query_weight: bfloat16 [2048, 1024], P(None, 'tp'), may hold values from -0.125 to 0.125
- key_weight: bfloat16 [2048, 1024], P(None, 'tp'), may hold values from -0.125 to 0.125
- value_weight: bfloat16 [2048, 1024], P(None, 'tp'), may hold values from -0.125 to 0.125
- outer_gate: bfloat16 [2048, 1024], P(None, 'tp'), may hold values from -0.125 to 0.125
- inner_gate: bfloat16 [2048, 1024], P(None, 'tp'), may hold values from -0.125 to 0.125
- conv_weight: bfloat16 [2048, 1024], P(None, 'tp'), may hold values from -0.125 to 0.125
- conv_taps: bfloat16 [3, 1024], P(None, 'tp'), may hold values from -3 to 3
- gate_sum: float32 [8, 24576], P('tp'), may hold values from -1412 to 0, as said below
- head_gain: bfloat16 [1024], P('tp'), may hold values from 0.099609375 to 1.8984375
- channel_gain: bfloat16 [1024], P('tp'), may hold values from 0.099609375 to 1.8984375
- attention_out: bfloat16 [1024, 2048], P('tp'), may hold values from -0.125 to 0.125
- channel_out: bfloat16 [1024, 2048], P('tp'), may hold values from -0.125 to 0.125
Outputs:
- mixed_out: bfloat16 [24576, 2048], P(('sp', 'tp'))
Inputs may be any that keep to these rules, and one draw needn't show every extreme that they name: gate_sum[h, t] never rises with t.
All inputs are finite; a program needn't handle non-finite values.
Results may differ from a plain program's by a relative error of at most 0.015.
Values may be sent and summed in bfloat16 or wider, within the bound.
No kernel may reach another device: no remote copies, remote signals or barrier semaphores. Data moves between devices by JAX's collectives and lax.ppermute only.
A program may use at most 192 MiB of HBM per device.

v0:
```python
import jax
import jax.numpy as jnp
from jax import lax
from jax.sharding import PartitionSpec as P

HEAD = 128
KTAP = 3


def laid_out(pieces, dim):
    pieces = jnp.moveaxis(pieces, 0, dim)
    lengths = pieces.shape
    return pieces.reshape(*lengths[:dim], lengths[dim] * lengths[dim + 1], *lengths[dim + 2 :])


def copy_for_each(shard, axis):
    peers = lax.axis_size(axis)
    return lax.all_to_all(
        jnp.broadcast_to(shard[None], (peers, *shard.shape)), axis, 0, 0, tiled=True
    )


def collect(shard, axis, dim):
    return laid_out(copy_for_each(shard, axis), dim)


def passed_along(shard, axis, by):
    peers = lax.axis_size(axis)
    pairs = [(i, i + by) for i in range(peers) if 0 <= i + by < peers]
    return lax.ppermute(shard, axis, pairs)


def sent_together(arrays, axis, dim, along):
    both = jnp.concatenate(arrays, axis=along)
    filled, at, gathered = (lax.all_gather(both, axis, axis=dim, tiled=True), 0, [])
    for a in arrays:
        gathered.append(lax.slice_in_dim(filled, at, at + a.shape[along], axis=along))
        at += a.shape[along]
    return tuple(gathered)


def head_norm(values, gain_vector):
    row_count = values.shape[0]
    shaped = values.reshape(row_count, -1, HEAD)
    shaped = shaped * lax.rsqrt(jnp.mean(shaped * shaped, axis=-1, keepdims=True) + 1e-06)
    return (shaped.reshape(row_count, -1) * gain_vector.astype(jnp.float32)).astype(jnp.bfloat16)


def block_size(total_rows, unit_rows):
    best_rows = unit_rows
    for factor in range(1, total_rows // unit_rows + 1):
        if total_rows // unit_rows % factor == 0 and factor * unit_rows <= 2048:
            best_rows = factor * unit_rows
    return best_rows


def local(
    tokens,
    query_weight,
    key_weight,
    value_weight,
    outer_gate,
    inner_gate,
    conv_weight,
    conv_taps,
    gate_sum,
    head_gain,
    channel_gain,
    attention_out,
    channel_out,
):
    weight_list = (query_weight, key_weight, value_weight, outer_gate, inner_gate, conv_weight)

    def project_rows(piece_rows):
        return jnp.concatenate(
            [
                jnp.dot(piece_rows, weight, preferred_element_type=jnp.float32).astype(jnp.bfloat16)
                for weight in weight_list
            ],
            axis=1,
        )

    projected = project_rows(collect(tokens, "tp", 0))
    pieces_list = []
    offset = 0
    for weight in weight_list:
        pieces_list.append(projected[:, offset : offset + weight.shape[1]])
        offset = offset + weight.shape[1]
    queries, keys_here, values_here, gate_outer, gate_inner, conv_input = pieces_list
    row_count = projected.shape[0]
    first_row = lax.axis_index("sp") * row_count
    mixed_in = (gate_inner.astype(jnp.float32) * conv_input.astype(jnp.float32)).astype(
        jnp.bfloat16
    )
    carried = passed_along(mixed_in[row_count - (KTAP - 1) :], "sp", 1)
    padded = jnp.concatenate([carried, mixed_in], axis=0).astype(jnp.float32)
    summed = jnp.zeros(mixed_in.shape, jnp.float32)
    for offset in range(KTAP):
        summed = (
            summed + conv_taps[offset].astype(jnp.float32) * padded[offset : offset + row_count]
        )
    conv_out = gate_outer.astype(jnp.float32) * summed
    heads_here = queries.shape[1] // HEAD
    query_heads = queries.reshape(row_count, heads_here, HEAD)
    query_gate = lax.dynamic_slice_in_dim(gate_sum, first_row, row_count, 1).T
    query_pos = first_row + jnp.arange(row_count, dtype=jnp.int32)
    last_row = first_row + row_count - 1
    score_scale = HEAD ** (-0.5)
    initial = (
        jnp.full((row_count, heads_here), -jnp.inf, jnp.float32),
        jnp.zeros((row_count, heads_here), jnp.float32),
        jnp.zeros((row_count, heads_here, HEAD), jnp.float32),
    )
    key_piece, value_piece = sent_together((keys_here, values_here), "sp", 0, 1)
    piece_length = key_piece.shape[0]
    span_rows = block_size(piece_length, row_count)

    def one_block(block_index, state_in):
        key_start = block_index * span_rows

        def work(state_old):
            peak_old, total_old, accum_old = state_old
            key_block = lax.dynamic_slice_in_dim(
                key_piece, block_index * span_rows, span_rows, 0
            ).reshape(span_rows, heads_here, HEAD)
            value_block = lax.dynamic_slice_in_dim(
                value_piece, block_index * span_rows, span_rows, 0
            ).reshape(span_rows, heads_here, HEAD)
            gate_block = lax.dynamic_slice_in_dim(gate_sum, key_start, span_rows, 1)
            logits = (
                jnp.einsum(
                    "qhd,khd->qhk", query_heads, key_block, preferred_element_type=jnp.float32
                )
                * score_scale
            )
            logits = logits + query_gate[:, :, None] - gate_block[None, :, :]
            key_pos = key_start + jnp.arange(span_rows, dtype=jnp.int32)
            allowed = (key_pos[None, :] <= query_pos[:, None])[:, None, :]
            peak_new = jnp.maximum(peak_old, jnp.max(jnp.where(allowed, logits, -jnp.inf), axis=-1))
            peak_safe = jnp.where(peak_new > -jnp.inf, peak_new, 0.0)
            weights = jnp.where(allowed, jnp.exp(logits - peak_safe[..., None]), 0.0)
            rescale = jnp.exp(peak_old - peak_safe)
            total_new = total_old * rescale + jnp.sum(weights, axis=-1)
            accum_new = accum_old * rescale[..., None] + jnp.einsum(
                "qhk,khd->qhd",
                weights.astype(jnp.bfloat16),
                value_block,
                preferred_element_type=jnp.float32,
            )
            return (peak_new, total_new, accum_new)

        return lax.cond(key_start <= last_row, work, lambda state_old: state_old, state_in)

    peak_end, total_end, accum_end = lax.fori_loop(0, piece_length // span_rows, one_block, initial)
    attention = (accum_end / total_end[..., None]).reshape(row_count, heads_here * HEAD)
    head_normed = head_norm(attention, head_gain)
    group_normed = head_norm(conv_out, channel_gain)
    att_all, group_all = (
        lax.all_to_all(head_normed, "tp", split_axis=0, concat_axis=1, tiled=True),
        lax.all_to_all(group_normed, "tp", split_axis=0, concat_axis=1, tiled=True),
    )
    att_piece, group_piece = sent_together((attention_out, channel_out), "tp", 0, 1)
    mixed_out = jnp.dot(att_all, att_piece, preferred_element_type=jnp.float32) + jnp.dot(
        group_all, group_piece, preferred_element_type=jnp.float32
    )
    return mixed_out.astype(jnp.bfloat16)


def solution(mesh):
    placed = (
        P(("sp", "tp"), None),
        P(None, "tp"),
        P(None, "tp"),
        P(None, "tp"),
        P(None, "tp"),
        P(None, "tp"),
        P(None, "tp"),
        P(None, "tp"),
        P("tp", None),
        P("tp"),
        P("tp"),
        P("tp", None),
        P("tp", None),
    )
    return jax.shard_map(
        local, mesh=mesh, in_specs=placed, out_specs=P(("sp", "tp"), None), check_vma=False
    )
```

profile of v0, /device:TPU:248, one launch (start us, length us, event | category | flops | bytes accessed | tf_op | source)
XLA Modules:
  0.0 303.0 jit_solution(9450191059030921678)
XLA Ops:
  7.9 24.8 %all_to_all.40 = bf16[4,96,2048]{2,1,0:T(8,128)(2,1)S(1)} all-to-all(bf16[4,96,2048]{2,1,0:T(8,128)(2,1)S(1)} %broadcast_in_dim.37), channel_id=1, replica_groups=mesh['sp'=64,'tp'=4] {'tp'}, dimensions={0} | all-to-all | bytes 3145728 | tf_op jit(solution)/shard_map/all_to_all | solution.py:18
  35.1 3.1 %pad_maximum_fusion = bf16[256,4096]{1,0:T(8,128)(2,1)} fusion(bf16[256,2048]{1,0:T(8,128)(2,1)} %param.29, bf16[256,2048]{1,0:T(8,128)(2,1)} %param.28), kind=kLoop, calls=%fused_computation.29 | loop fusion | flops 4194304 | bytes 4194304 | tf_op jit(solution)/shard_map/concatenate | solution.py:34
  38.3 1.8 fusion.29
  40.1 1.8 fusion.32
  42.0 1.9 collective-permute-start
  44.6 2.3 collective-permute-done
  49.4 3.4 %all-to-all-start.2 = ((bf16[4,96,256]{2,1,0:T(8,128)(2,1)}), bf16[4,96,256]{2,1,0:T(8,128)(2,1)S(1)}, u32[]{:S(2)}, u32[]{:S(2)}) async-start(bf16[4,96,256]{2,1,0:T(8,128)(2,1)} %bitcast.11), calls=%async_computation.2 | async-start | bytes 393216 | tf_op jit(solution)/shard_map/all_to_all | solution.py:160
  52.8 2.0 convolution_convert_fusion.3
  55.0 4.1 %all-to-all-done.2 = bf16[4,96,256]{2,1,0:T(8,128)(2,1)S(1)} async-done(((bf16[4,96,256]{2,1,0:T(8,128)(2,1)}), bf16[4,96,256]{2,1,0:T(8,128)(2,1)S(1)}, u32[]{:S(2)}, u32[]{:S(2)}) %all-to-all-start.2) | async-done | bytes 196640 | tf_op jit(solution)/shard_map/all_to_all | solution.py:160
  59.1 101.1 %all-gather.3.cloned.1.call-done = bf16[24576,512]{0,1:T(8,128)(2,1)} async-done(((bf16[384,512]{0,1:T(8,128)(2,1)}), bf16[24576,512]{0,1:T(8,128)(2,1)}) %all-gather.3.cloned.1.call-update) | async-done | bytes 25165840 | tf_op jit(solution)/shard_map/all_gather | solution.py:35
  160.2 17.9 %fusion.37 = (bf16[24576,256]{0,1:T(8,128)(2,1)}, bf16[24576,256]{0,1:T(8,128)(2,1)}) fusion(bf16[24576,512]{0,1:T(8,128)(2,1)} %all-gather.3.cloned.1.call-done), kind=kLoop, calls=%fused_computation.62 | loop fusion | bytes 50331648 | tf_op jit(solution)/shard_map/slice | solution.py:37
  178.2 102.2 %while.18 = (s32[]{:T(128)}, f32[384,2]{0,1:T(2,128)S(1)}, f32[384,2]{0,1:T(2,128)S(1)}, f32[384,2,128]{0,2,1:T(8,128)S(1)}, s32[]{:T(128)}, /*index=5*/bf16[245...) while((s32[]{:T(128)}, f32[384,2]{0,1:T(2,128)S(1)}, ...), condition=%wide.region_5.6_spmd.clone, body=%wide.region_0.5_spmd.clone.sunk | while | flops 617748864 | bytes 22327696 | solution.py:154
  178.2 6.5 %conditional.3 = ((f32[384,2]{0,1:T(2,128)S(1)}, f32[384,2]{0,1:T(2,128)S(1)}, f32[384,2,128]{0,2,1:T(8,128)S(1)})) conditional(s32[]{:T(128)} %convert_element_type.121, (f32[384,2]{0,1:T(2,128)S(1)}, f32[384,2]{0,1:T(2,128)S(1)}, f32[384,2,128]{0,2,1:T(8,128)S(1)}) %tuple.54, (s32[]{:T(128)}, s32[]{:T(128)}, s32[]{:T(128)}, ...), branch_computations={%region_1.0_spmd, %region_2.4_spmd} | conditional | flops 617748864 | bytes 22325888 | solution.py:152
  184.7 6.3 %conditional.3 = ((f32[384,2]{0,1:T(2,128)S(1)}, f32[384,2]{0,1:T(2,128)S(1)}, f32[384,2,128]{0,2,1:T(8,128)S(1)})) conditional(s32[]{:T(128)} %convert_element_type.121, (f32[384,2]{0,1:T(2,128)S(1)}, f32[384,2]{0,1:T(2,128)S(1)}, f32[384,2,128]{0,2,1:T(8,128)S(1)}) %tuple.54, (s32[]{:T(128)}, s32[]{:T(128)}, s32[]{:T(128)}, ...), branch_computations={%region_1.0_spmd, %region_2.4_spmd} | conditional | flops 617748864 | bytes 22325888 | solution.py:152
  191.1 6.3 %conditional.3 = ((f32[384,2]{0,1:T(2,128)S(1)}, f32[384,2]{0,1:T(2,128)S(1)}, f32[384,2,128]{0,2,1:T(8,128)S(1)})) conditional(s32[]{:T(128)} %convert_element_type.121, (f32[384,2]{0,1:T(2,128)S(1)}, f32[384,2]{0,1:T(2,128)S(1)}, f32[384,2,128]{0,2,1:T(8,128)S(1)}) %tuple.54, (s32[]{:T(128)}, s32[]{:T(128)}, s32[]{:T(128)}, ...), branch_computations={%region_1.0_spmd, %region_2.4_spmd} | conditional | flops 617748864 | bytes 22325888 | solution.py:152
  197.5 6.4 %conditional.3 = ((f32[384,2]{0,1:T(2,128)S(1)}, f32[384,2]{0,1:T(2,128)S(1)}, f32[384,2,128]{0,2,1:T(8,128)S(1)})) conditional(s32[]{:T(128)} %convert_element_type.121, (f32[384,2]{0,1:T(2,128)S(1)}, f32[384,2]{0,1:T(2,128)S(1)}, f32[384,2,128]{0,2,1:T(8,128)S(1)}) %tuple.54, (s32[]{:T(128)}, s32[]{:T(128)}, s32[]{:T(128)}, ...), branch_computations={%region_1.0_spmd, %region_2.4_spmd} | conditional | flops 617748864 | bytes 22325888 | solution.py:152
  203.9 6.4 %conditional.3 = ((f32[384,2]{0,1:T(2,128)S(1)}, f32[384,2]{0,1:T(2,128)S(1)}, f32[384,2,128]{0,2,1:T(8,128)S(1)})) conditional(s32[]{:T(128)} %convert_element_type.121, (f32[384,2]{0,1:T(2,128)S(1)}, f32[384,2]{0,1:T(2,128)S(1)}, f32[384,2,128]{0,2,1:T(8,128)S(1)}) %tuple.54, (s32[]{:T(128)}, s32[]{:T(128)}, s32[]{:T(128)}, ...), branch_computations={%region_1.0_spmd, %region_2.4_spmd} | conditional | flops 617748864 | bytes 22325888 | solution.py:152
  210.3 6.4 %conditional.3 = ((f32[384,2]{0,1:T(2,128)S(1)}, f32[384,2]{0,1:T(2,128)S(1)}, f32[384,2,128]{0,2,1:T(8,128)S(1)})) conditional(s32[]{:T(128)} %convert_element_type.121, (f32[384,2]{0,1:T(2,128)S(1)}, f32[384,2]{0,1:T(2,128)S(1)}, f32[384,2,128]{0,2,1:T(8,128)S(1)}) %tuple.54, (s32[]{:T(128)}, s32[]{:T(128)}, s32[]{:T(128)}, ...), branch_computations={%region_1.0_spmd, %region_2.4_spmd} | conditional | flops 617748864 | bytes 22325888 | solution.py:152
  216.7 6.3 %conditional.3 = ((f32[384,2]{0,1:T(2,128)S(1)}, f32[384,2]{0,1:T(2,128)S(1)}, f32[384,2,128]{0,2,1:T(8,128)S(1)})) conditional(s32[]{:T(128)} %convert_element_type.121, (f32[384,2]{0,1:T(2,128)S(1)}, f32[384,2]{0,1:T(2,128)S(1)}, f32[384,2,128]{0,2,1:T(8,128)S(1)}) %tuple.54, (s32[]{:T(128)}, s32[]{:T(128)}, s32[]{:T(128)}, ...), branch_computations={%region_1.0_spmd, %region_2.4_spmd} | conditional | flops 617748864 | bytes 22325888 | solution.py:152
  223.1 6.3 %conditional.3 = ((f32[384,2]{0,1:T(2,128)S(1)}, f32[384,2]{0,1:T(2,128)S(1)}, f32[384,2,128]{0,2,1:T(8,128)S(1)})) conditional(s32[]{:T(128)} %convert_element_type.121, (f32[384,2]{0,1:T(2,128)S(1)}, f32[384,2]{0,1:T(2,128)S(1)}, f32[384,2,128]{0,2,1:T(8,128)S(1)}) %tuple.54, (s32[]{:T(128)}, s32[]{:T(128)}, s32[]{:T(128)}, ...), branch_computations={%region_1.0_spmd, %region_2.4_spmd} | conditional | flops 617748864 | bytes 22325888 | solution.py:152
  229.5 6.3 %conditional.3 = ((f32[384,2]{0,1:T(2,128)S(1)}, f32[384,2]{0,1:T(2,128)S(1)}, f32[384,2,128]{0,2,1:T(8,128)S(1)})) conditional(s32[]{:T(128)} %convert_element_type.121, (f32[384,2]{0,1:T(2,128)S(1)}, f32[384,2]{0,1:T(2,128)S(1)}, f32[384,2,128]{0,2,1:T(8,128)S(1)}) %tuple.54, (s32[]{:T(128)}, s32[]{:T(128)}, s32[]{:T(128)}, ...), branch_computations={%region_1.0_spmd, %region_2.4_spmd} | conditional | flops 617748864 | bytes 22325888 | solution.py:152
  235.8 6.3 %conditional.3 = ((f32[384,2]{0,1:T(2,128)S(1)}, f32[384,2]{0,1:T(2,128)S(1)}, f32[384,2,128]{0,2,1:T(8,128)S(1)})) conditional(s32[]{:T(128)} %convert_element_type.121, (f32[384,2]{0,1:T(2,128)S(1)}, f32[384,2]{0,1:T(2,128)S(1)}, f32[384,2,128]{0,2,1:T(8,128)S(1)}) %tuple.54, (s32[]{:T(128)}, s32[]{:T(128)}, s32[]{:T(128)}, ...), branch_computations={%region_1.0_spmd, %region_2.4_spmd} | conditional | flops 617748864 | bytes 22325888 | solution.py:152
  242.2 6.3 %conditional.3 = ((f32[384,2]{0,1:T(2,128)S(1)}, f32[384,2]{0,1:T(2,128)S(1)}, f32[384,2,128]{0,2,1:T(8,128)S(1)})) conditional(s32[]{:T(128)} %convert_element_type.121, (f32[384,2]{0,1:T(2,128)S(1)}, f32[384,2]{0,1:T(2,128)S(1)}, f32[384,2,128]{0,2,1:T(8,128)S(1)}) %tuple.54, (s32[]{:T(128)}, s32[]{:T(128)}, s32[]{:T(128)}, ...), branch_computations={%region_1.0_spmd, %region_2.4_spmd} | conditional | flops 617748864 | bytes 22325888 | solution.py:152
  248.6 6.3 %conditional.3 = ((f32[384,2]{0,1:T(2,128)S(1)}, f32[384,2]{0,1:T(2,128)S(1)}, f32[384,2,128]{0,2,1:T(8,128)S(1)})) conditional(s32[]{:T(128)} %convert_element_type.121, (f32[384,2]{0,1:T(2,128)S(1)}, f32[384,2]{0,1:T(2,128)S(1)}, f32[384,2,128]{0,2,1:T(8,128)S(1)}) %tuple.54, (s32[]{:T(128)}, s32[]{:T(128)}, s32[]{:T(128)}, ...), branch_computations={%region_1.0_spmd, %region_2.4_spmd} | conditional | flops 617748864 | bytes 22325888 | solution.py:152
  255.0 6.3 %conditional.3 = ((f32[384,2]{0,1:T(2,128)S(1)}, f32[384,2]{0,1:T(2,128)S(1)}, f32[384,2,128]{0,2,1:T(8,128)S(1)})) conditional(s32[]{:T(128)} %convert_element_type.121, (f32[384,2]{0,1:T(2,128)S(1)}, f32[384,2]{0,1:T(2,128)S(1)}, f32[384,2,128]{0,2,1:T(8,128)S(1)}) %tuple.54, (s32[]{:T(128)}, s32[]{:T(128)}, s32[]{:T(128)}, ...), branch_computations={%region_1.0_spmd, %region_2.4_spmd} | conditional | flops 617748864 | bytes 22325888 | solution.py:152
  261.3 6.3 %conditional.3 = ((f32[384,2]{0,1:T(2,128)S(1)}, f32[384,2]{0,1:T(2,128)S(1)}, f32[384,2,128]{0,2,1:T(8,128)S(1)})) conditional(s32[]{:T(128)} %convert_element_type.121, (f32[384,2]{0,1:T(2,128)S(1)}, f32[384,2]{0,1:T(2,128)S(1)}, f32[384,2,128]{0,2,1:T(8,128)S(1)}) %tuple.54, (s32[]{:T(128)}, s32[]{:T(128)}, s32[]{:T(128)}, ...), branch_computations={%region_1.0_spmd, %region_2.4_spmd} | conditional | flops 617748864 | bytes 22325888 | solution.py:152
  267.7 6.3 %conditional.3 = ((f32[384,2]{0,1:T(2,128)S(1)}, f32[384,2]{0,1:T(2,128)S(1)}, f32[384,2,128]{0,2,1:T(8,128)S(1)})) conditional(s32[]{:T(128)} %convert_element_type.121, (f32[384,2]{0,1:T(2,128)S(1)}, f32[384,2]{0,1:T(2,128)S(1)}, f32[384,2,128]{0,2,1:T(8,128)S(1)}) %tuple.54, (s32[]{:T(128)}, s32[]{:T(128)}, s32[]{:T(128)}, ...), branch_computations={%region_1.0_spmd, %region_2.4_spmd} | conditional | flops 617748864 | bytes 22325888 | solution.py:152
  274.1 6.3 %conditional.3 = ((f32[384,2]{0,1:T(2,128)S(1)}, f32[384,2]{0,1:T(2,128)S(1)}, f32[384,2,128]{0,2,1:T(8,128)S(1)})) conditional(s32[]{:T(128)} %convert_element_type.121, (f32[384,2]{0,1:T(2,128)S(1)}, f32[384,2]{0,1:T(2,128)S(1)}, f32[384,2,128]{0,2,1:T(8,128)S(1)}) %tuple.54, (s32[]{:T(128)}, s32[]{:T(128)}, s32[]{:T(128)}, ...), branch_computations={%region_1.0_spmd, %region_2.4_spmd} | conditional | flops 617748864 | bytes 22325888 | solution.py:152
  281.8 4.2 %all-to-all-start.1 = ((bf16[4,96,256]{2,1,0:T(8,128)(2,1)}), bf16[4,96,256]{2,1,0:T(8,128)(2,1)S(1)}, u32[]{:S(2)}, u32[]{:S(2)}) async-start(bf16[4,96,256]{2,1,0:T(8,128)(2,1)} %multiply_convert_fusion), calls=%async_computation.1 | async-start | bytes 393216 | tf_op jit(solution)/shard_map/all_to_all | solution.py:159
  286.0 3.1 %fusion.17 = f32[96,2048]{1,0:T(8,128)S(1)} fusion(bf16[96,1024]{1,0:T(8,128)(2,1)S(1)} %bitcast.60, bf16[1024,4096]{1,0:T(8,128)(2,1)} %all-gather.5.cloned.1.call-done), kind=kOutput, calls=%fused_computation.23 | convolution fusion | flops 402653184 | bytes 5177344 | tf_op jit(solution)/shard_map/dot_general | solution.py:163
  289.1 3.3 %all-to-all-done.1 = bf16[4,96,256]{2,1,0:T(8,128)(2,1)S(1)} async-done(((bf16[4,96,256]{2,1,0:T(8,128)(2,1)}), bf16[4,96,256]{2,1,0:T(8,128)(2,1)S(1)}, u32[]{:S(2)}, u32[]{:S(2)}) %all-to-all-start.1) | async-done | bytes 196640 | tf_op jit(solution)/shard_map/all_to_all | solution.py:159
  292.4 3.7 %fusion.24 = bf16[96,2048]{1,0:T(8,128)(2,1)} fusion(f32[96,2048]{1,0:T(8,128)S(1)} %fusion.17, bf16[96,1024]{1,0:T(8,128)(2,1)S(1)} %bitcast.61, bf16[1024,4096]{1,0:T(8,128)(2,1)} %all-gather.5.cloned.1.call-done), kind=kOutput, calls=%fused_computation.28 | convolution fusion | flops 403046400 | bytes 5570560 | tf_op jit(solution)/shard_map/dot_general | solution.py:163
  (239 shorter events, 109.0 us)
Async XLA Ops:
  6.5 40.4 %copy-start = (bf16[2048,256]{1,0:T(8,128)(2,1)S(1)}, bf16[2048,256]{1,0:T(8,128)(2,1)}, u32[]{:S(2)}) copy-start(bf16[2048,256]{1,0:T(8,128)(2,1)} %param.21) | copy-start | bytes 3145732
  6.5 153.7 %all-gather.3.cloned.1.call-start = ((), (), s32[]{:S(2)}) async-start(), calls=%async_computation.3 | async-start | bytes 25559040 | tf_op jit(solution)/shard_map/all_gather | solution.py:35
  6.5 26.1 %copy-start.2 = (bf16[2048,256]{1,0:T(8,128)(2,1)S(1)}, bf16[2048,256]{1,0:T(8,128)(2,1)}, u32[]{:S(2)}) copy-start(bf16[2048,256]{1,0:T(8,128)(2,1)} %param.20) | copy-start | bytes 3145732
  6.5 26.9 %copy-start.3 = (bf16[2048,256]{1,0:T(8,128)(2,1)S(1)}, bf16[2048,256]{1,0:T(8,128)(2,1)}, u32[]{:S(2)}) copy-start(bf16[2048,256]{1,0:T(8,128)(2,1)} %param.19) | copy-start | bytes 3145732
  34.2 4.1 %copy-start.4 = (bf16[3,256]{1,0:T(4,128)(2,1)S(1)}, bf16[3,256]{1,0:T(4,128)(2,1)}, u32[]{:S(2)}) copy-start(bf16[3,256]{1,0:T(4,128)(2,1)} %param.24) | copy-start | bytes 4612
  35.1 251.0 %all-gather.5.cloned.1.call-start = ((), (), s32[]{:S(2)}) async-start(), calls=%async_computation.4 | async-start | bytes 10485760 | tf_op jit(solution)/shard_map/all_gather | solution.py:35
  38.3 6.3 %copy-start.5 = (bf16[256]{0:T(256)(128)(2,1)S(1)}, bf16[256]{0:T(256)(128)(2,1)}, u32[]{:S(2)}) copy-start(bf16[256]{0:T(256)(128)(2,1)} %param.26) | copy-start | bytes 1540
  38.3 6.3 %copy-start.6 = (bf16[256]{0:T(256)(128)(2,1)S(1)}, bf16[256]{0:T(256)(128)(2,1)}, u32[]{:S(2)}) copy-start(bf16[256]{0:T(256)(128)(2,1)} %param.27) | copy-start | bytes 1540
  42.0 4.9 %collective-permute-start = (bf16[2,256]{1,0:T(2,128)(2,1)S(1)}, bf16[2,256]{1,0:T(2,128)(2,1)S(1)}, u32[]{:S(2)}, u32[]{:S(2)}) collective-permute-start(bf16[2,256]{1,0:T(2,128)(2,1)S(1)} %slice.47), channel_id=1, source_target_pairs={{0,4},{4,8},{8,12},{12,16},{16,20},{20,24},{24,28},{28,32},{32,36}... | collective-permute-start | bytes 3080 | tf_op jit(solution)/shard_map/ppermute | solution.py:30
  49.4 9.7 %all-to-all-start.2 = ((bf16[4,96,256]{2,1,0:T(8,128)(2,1)}), bf16[4,96,256]{2,1,0:T(8,128)(2,1)S(1)}, u32[]{:S(2)}, u32[]{:S(2)}) async-start(bf16[4,96,256]{2,1,0:T(8,128)(2,1)} %bitcast.11), calls=%async_computation.2 | async-start | bytes 393216 | tf_op jit(solution)/shard_map/all_to_all | solution.py:160
  281.8 10.6 %all-to-all-start.1 = ((bf16[4,96,256]{2,1,0:T(8,128)(2,1)}), bf16[4,96,256]{2,1,0:T(8,128)(2,1)S(1)}, u32[]{:S(2)}, u32[]{:S(2)}) async-start(bf16[4,96,256]{2,1,0:T(8,128)(2,1)} %multiply_convert_fusion), calls=%async_computation.1 | async-start | bytes 393216 | tf_op jit(solution)/shard_map/all_to_all | solution.py:159
  286.0 10.1 %copy-start.1 = (bf16[2048,256]{1,0:T(8,128)(2,1)S(1)}, bf16[2048,256]{1,0:T(8,128)(2,1)}, u32[]{:S(2)}) copy-start(bf16[2048,256]{1,0:T(8,128)(2,1)} %param.21) | copy-start | bytes 3145732
Sparse Core Ops, SparseCore 0:
  35.2 124.9 all-gather.2
  162.0 85.8 all-gather.4
where the time goes:
time: 305 us; the launch traced here: 303 us
  waiting for transfers between devices  111 us (36%)
  matrix products  58 us (19%)
  local copies, waits for them, and re-layouts  56.7 us (19%)
  other arithmetic  27.7 us (9%)
  blocking collectives  24.8 us (8%)
  between operations  13.7 us (4%)
  starting transfers between devices  9.58 us (3%)
    all_gather x2, waiting for transfers between devices, sent_together(): lax.all_gather(both, axis, axis=dim, tiled=True)  101 us
    all_to_all x1, blocking collectives, copy_for_each(): lax.all_to_all(jnp.broadcast_to(shard[None], (peers, *shard.shape)), axis...  24.8 us
    dot_general x16, matrix products, work(): jnp.einsum('qhd,khd->qhk', query_heads, key_block, preferred_element_type...  24.2 us
    dynamic_slice x16, local copies, waits for them, and re-layouts, work(): lax.dynamic_slice_in_dim(value_piece, block_index * span_rows, span_rows, 0)  23.8 us
    dot_general x16, matrix products, work(): jnp.einsum('qhk,khd->qhd', weights.astype(jnp.bfloat16), value_block, pre...  19.3 us
    slice x1, local copies, waits for them, and re-layouts, sent_together(): lax.slice_in_dim(filled, at, at + a.shape[along], axis=along)  17.9 us
    reduce_sum x16, other arithmetic, work(): total_new = total_old * rescale + jnp.sum(weights, axis=-1)  15 us
    dynamic_slice x16, local copies, waits for them, and re-layouts, work(): gate_block = lax.dynamic_slice_in_dim(gate_sum, key_start, span_rows, 1)  11.4 us
  transfers between devices with their start and end apart: 5, of which 4 were waited for; matrix products, arithmetic and copies ran while one was open for 45% of the time, Pallas kernels for 0%

commit v1 on v0

v1 whole, which is shorter than its diff:
```python
import jax
import jax.numpy as jnp
from jax import lax
from jax.experimental import pallas as pl
from jax.experimental.pallas import tpu as pltpu
from jax.sharding import Mesh
from jax.sharding import PartitionSpec as P

HEAD = 128
KTAP = 3
LOG2E = 1.4426950408889634
LOW = -1e30
EPS = 1e-06
BF = jnp.bfloat16
F32 = jnp.float32

NZ, NY, NC, NX = 8, 4, 2, 4
OWN = 384
CHUNK = NC * OWN
ROWS = OWN // NX
STAT = 16
SUB = 128


def shifted(a, axis, by):
    n = lax.axis_size(axis)
    return lax.ppermute(a, axis, [(i, (i + by) % n) for i in range(n)])


def dot(a, b):
    return jnp.dot(a, b, preferred_element_type=F32)


def update(q, kv, gate, m, l, acc, masked):
    keys, values = kv[:, :HEAD], kv[:, HEAD:]
    s = lax.dot_general(q, keys, (((1,), (1,)), ((), ())), preferred_element_type=F32)
    n = s.shape[1] // HEAD
    scale = HEAD**-0.5 * LOG2E
    parts = []
    for j in range(n):
        part = s[:, j * HEAD : (j + 1) * HEAD] * scale - gate[:, j * HEAD : (j + 1) * HEAD]
        if masked is not None:
            part = jnp.where(masked(j), part, LOW)
        parts.append(part)
    top = parts[0]
    for part in parts[1:]:
        top = jnp.maximum(top, part)
    m_new = jnp.maximum(m, jnp.max(top, axis=1, keepdims=True))
    alpha = jnp.exp2(m - m_new)
    total = l * alpha
    probs = []
    for part in parts:
        p = jnp.exp2(part - m_new)
        total = total + p
        probs.append(p.astype(BF))
    p_all = jnp.concatenate(probs, axis=1)
    acc_new = acc * alpha + dot(p_all, values)
    return m_new, total, acc_new


def first_kernel(code_ref, q_ref, kv_ref, g_ref, m_ref, l_ref, a_ref):
    tile = pl.program_id(0)
    code = code_ref[tile // NC]
    core = code_ref[NY]
    half = tile % NC
    zidx = code_ref[NY + 1]

    @pl.when(code == 0)
    def _():
        m_ref[...] = jnp.full(m_ref.shape, LOW, F32)
        l_ref[...] = jnp.zeros(l_ref.shape, F32)
        a_ref[...] = jnp.zeros(a_ref.shape, F32)

    def run(diag):
        for r in range(OWN // SUB):
            rows = slice(r * SUB, (r + 1) * SUB)
            masked = None
            if diag:
                first = (half * OWN + core * OWN) % CHUNK + r * SUB

                def masked(j):
                    qpos = first + lax.broadcasted_iota(jnp.int32, (SUB, HEAD), 0)
                    kfirst = (j * HEAD + core * OWN) % CHUNK
                    kpos = kfirst + lax.broadcasted_iota(jnp.int32, (SUB, HEAD), 1)
                    return kpos <= qpos

            zero = jnp.zeros((SUB, HEAD), F32)
            m, l, a = update(
                q_ref[rows], kv_ref[...], g_ref[zidx], jnp.full((SUB, HEAD), LOW, F32), zero, zero, masked
            )
            m_ref[rows] = m
            l_ref[rows] = l
            a_ref[rows] = a

    pl.when(code == 1)(lambda: run(False))
    pl.when(code == 2)(lambda: run(True))


def next_kernel(flag_ref, q_ref, kva_ref, kvb_ref, ga_ref, gb_ref, mi, li, ai, mo, lo, ao):
    mo[...] = mi[...]
    lo[...] = li[...]
    ao[...] = ai[...]

    def run(kv_ref, g_ref, zidx):
        for r in range(OWN // SUB):
            rows = slice(r * SUB, (r + 1) * SUB)
            m, l, a = update(q_ref[rows], kv_ref[...], g_ref[zidx], mo[rows], lo[rows], ao[rows], None)
            mo[rows] = m
            lo[rows] = l
            ao[rows] = a

    pl.when(flag_ref[0] == 1)(lambda: run(kva_ref, ga_ref, flag_ref[2]))
    pl.when(flag_ref[1] == 1)(lambda: run(kvb_ref, gb_ref, flag_ref[3]))


def finish(m, l, acc, out_ref):
    total = jnp.sum(l, axis=1, keepdims=True)
    some = total > 0.0
    safe = jnp.where(some, total, 1.0)
    out = (acc / safe).astype(BF)
    lse = jnp.where(some, m + jnp.log2(safe), LOW)
    row = lax.broadcasted_iota(jnp.int32, (ROWS, HEAD), 0)
    lane = lax.broadcasted_iota(jnp.int32, (ROWS, HEAD), 1)
    for b in range(NX):
        rows = slice(b * ROWS, (b + 1) * ROWS)
        out_ref[0, 0, b, :ROWS, :] = out[rows]
        line = jnp.sum(jnp.where(row == lane, lse[rows], 0.0), axis=0, keepdims=True)
        high = line.astype(BF)
        rest = line - high.astype(F32)
        mid = rest.astype(BF)
        low = (rest - mid.astype(F32)).astype(BF)
        out_ref[0, 0, b, ROWS:, :] = jnp.concatenate(
            [high.astype(F32), mid.astype(F32), low.astype(F32), jnp.zeros((STAT - 3, HEAD), F32)], axis=0
        ).astype(BF)


def last_kernel(flag_ref, q_ref, kva_ref, kvb_ref, ga_ref, gb_ref, mi, li, ai, out_ref, mo, lo, ao):
    next_kernel(flag_ref, q_ref, kva_ref, kvb_ref, ga_ref, gb_ref, mi, li, ai, mo, lo, ao)
    finish(mo[...], lo[...], ao[...], out_ref)


def attention_cost(keys):
    rows = NY * CHUNK
    return pl.CostEstimate(
        flops=rows * keys * HEAD * 4, transcendentals=rows * keys, bytes_accessed=rows * HEAD * 26
    )


STATE = jax.ShapeDtypeStruct((NY * CHUNK, HEAD), F32)
TILES = NY * CHUNK // OWN


def tile_spec():
    return pl.BlockSpec((OWN, HEAD), lambda i, *_: (i, 0))


def whole(a):
    return pl.BlockSpec(a.shape, lambda i, *_, n=a.ndim: (0,) * n)


def attend_first(code, q, kv, gate):
    return pl.pallas_call(
        first_kernel,
        grid_spec=pltpu.PrefetchScalarGridSpec(
            num_scalar_prefetch=1,
            grid=(TILES,),
            in_specs=[tile_spec(), whole(kv), whole(gate)],
            out_specs=[tile_spec()] * 3,
        ),
        out_shape=[STATE] * 3,
        cost_estimate=attention_cost(CHUNK),
        name="attend_first",
    )(code, q, kv, gate)


def attend_next(flags, q, kva, kvb, ga, gb, state):
    return pl.pallas_call(
        next_kernel,
        grid_spec=pltpu.PrefetchScalarGridSpec(
            num_scalar_prefetch=1,
            grid=(TILES,),
            in_specs=[tile_spec(), whole(kva), whole(kvb), whole(ga), whole(gb)] + [tile_spec()] * 3,
            out_specs=[tile_spec()] * 3,
        ),
        out_shape=[STATE] * 3,
        input_output_aliases={6: 0, 7: 1, 8: 2},
        cost_estimate=attention_cost(CHUNK),
        name="attend_next",
    )(flags, q, kva, kvb, ga, gb, *state)


def attend_last(flags, q, kva, kvb, ga, gb, state):
    block = (1, 1, NX, ROWS + STAT, HEAD)

    def placed(i, flags):
        return (flags[4 + i // NC], flags[8 + i % NC], 0, 0, 0)

    return pl.pallas_call(
        last_kernel,
        grid_spec=pltpu.PrefetchScalarGridSpec(
            num_scalar_prefetch=1,
            grid=(TILES,),
            in_specs=[tile_spec(), whole(kva), whole(kvb), whole(ga), whole(gb)] + [tile_spec()] * 3,
            out_specs=pl.BlockSpec(block, placed),
            scratch_shapes=[pltpu.VMEM((OWN, HEAD), F32)] * 3,
        ),
        out_shape=jax.ShapeDtypeStruct((NY, NC, NX, ROWS + STAT, HEAD), BF),
        cost_estimate=attention_cost(CHUNK),
        name="attend_last",
    )(flags, q, kva, kvb, ga, gb, *state)


def merge_kernel(where_ref, part_ref, gain_ref, out_ref):
    row = lax.broadcasted_iota(jnp.int32, (ROWS, HEAD), 0)
    lane = lax.broadcasted_iota(jnp.int32, (ROWS, HEAD), 1)
    for c in range(NC):
        sums, outs = [], []
        for y in range(NY):
            stats = part_ref[y, c, 0, ROWS:, :].astype(F32)
            line = stats[0:1] + stats[1:2] + stats[2:3]
            sums.append(jnp.sum(jnp.where(row == lane, line, 0.0), axis=1, keepdims=True))
            outs.append(part_ref[y, c, 0, :ROWS, :].astype(F32))
        top = jnp.maximum(jnp.maximum(sums[0], sums[1]), jnp.maximum(sums[2], sums[3]))
        weights = [jnp.exp2(s - top) for s in sums]
        total = weights[0] + weights[1] + weights[2] + weights[3]
        mixed = (
            outs[0] * weights[0] + outs[1] * weights[1] + outs[2] * weights[2] + outs[3] * weights[3]
        ) / total
        mixed = mixed * lax.rsqrt(jnp.mean(mixed * mixed, axis=1, keepdims=True) + EPS)
        gain = gain_ref[0, 0:1, c * HEAD : (c + 1) * HEAD].astype(F32)
        out_ref[0, :, c * HEAD : (c + 1) * HEAD] = (mixed * gain).astype(BF)


def merge(where, parts, gains):
    return pl.pallas_call(
        merge_kernel,
        grid_spec=pltpu.PrefetchScalarGridSpec(
            num_scalar_prefetch=1,
            grid=(NX,),
            in_specs=[
                pl.BlockSpec((NY, NC, 1, ROWS + STAT, HEAD), lambda i, w: (0, 0, w[i], 0, 0)),
                pl.BlockSpec((1, STAT, NC * HEAD), lambda i, w: (i, 0, 0)),
            ],
            out_specs=pl.BlockSpec((1, ROWS, NC * HEAD), lambda i, w: (i, 0, 0)),
        ),
        out_shape=jax.ShapeDtypeStruct((NX, ROWS, NC * HEAD), BF),
        name="merge",
    )(where, parts, gains)


def group_norm(values, gain):
    count = values.shape[0]
    shaped = values.reshape(count, -1, HEAD)
    shaped = shaped * lax.rsqrt(jnp.mean(shaped * shaped, axis=-1, keepdims=True) + EPS)
    return (shaped.reshape(count, -1) * gain.astype(F32)).astype(BF)


def local(
    tokens, query_weight, key_weight, value_weight, outer_gate, inner_gate, conv_weight, conv_taps,
    gate_sum, head_gain, channel_gain, attention_out, channel_out,
):
    z, y, c, x = (lax.axis_index(a) for a in "zycx")
    other = 1 - c

    def head_of(weight, core):
        return lax.dynamic_slice_in_dim(weight, core * HEAD, HEAD, 1)

    from_left = shifted(tokens, "x", 1)
    from_right = shifted(tokens, "x", -1)
    half = ROWS // 2
    far_top = shifted(from_left[:half], "x", 1)
    far_low = shifted(from_right[half:], "x", -1)
    attn_weights = jnp.concatenate(
        [head_of(w, core) for core in (c, other) for w in (query_weight, key_weight, value_weight)], axis=1
    )
    conv_weights = jnp.concatenate([outer_gate, inner_gate, conv_weight], axis=1)
    pieces = [tokens, jnp.concatenate([from_left, from_right]), jnp.concatenate([far_top, far_low])]
    places = [[x], [(x + NX - 1) % NX, (x + 1) % NX], [(x + 2) % NX]]

    def project(weights):
        rows = jnp.zeros((NX, ROWS, weights.shape[1]), BF)
        for piece, at in zip(pieces, places):
            made = dot(piece, weights).astype(BF)
            for n, place in enumerate(at):
                rows = lax.dynamic_update_slice(rows, made[None, n * ROWS : (n + 1) * ROWS], (place, 0, 0))
        return rows.reshape(OWN, weights.shape[1])

    attn = project(attn_weights)
    mine = attn[:, : 3 * HEAD]
    got = shifted(attn[:, 3 * HEAD :], "c", 1)
    both = jnp.concatenate([mine, got], axis=0)
    q_own, kv_own = both[:, :HEAD], both[:, HEAD:]

    up, down = [kv_own], [kv_own]
    for _ in range(3):
        up.append(shifted(up[-1], "z", 1))
        down.append(shifted(down[-1], "z", -1))
    up_half = shifted(up[3][:OWN], "z", 1)
    down_half = shifted(down[3][OWN:], "z", -1)
    q_all = jnp.concatenate([q_own, shifted(q_own, "y", 1), shifted(q_own, "y", -1), shifted(q_own, "y", 2)])
    slots = jnp.stack([y, (y + NY - 1) % NY, (y + 1) % NY, (y + 2) % NY])

    gate = lax.dynamic_slice_in_dim(gate_sum, c, 1, 0).reshape(NZ, NY, NC, OWN)
    gate = lax.dynamic_index_in_dim(gate, y, 1, keepdims=False)
    gate = jnp.concatenate(
        [lax.dynamic_index_in_dim(gate, c, 1, keepdims=False), lax.dynamic_index_in_dim(gate, other, 1, keepdims=False)],
        axis=1,
    )
    gate = (gate * LOG2E)[:, None, :]

    code = jnp.concatenate([jnp.where(slots == y, 2, jnp.where(slots > y, 1, 0)), jnp.stack([c, z])]).astype(jnp.int32)
    state = attend_first(code, q_all, kv_own, gate)
    cores = jnp.stack([c, other])

    def flags_of(step):
        return jnp.concatenate(
            [
                jnp.stack([(z >= step).astype(jnp.int32), (z + step >= NZ).astype(jnp.int32)]),
                jnp.stack([(z + NZ - step) % NZ, (z + step) % NZ]),
                slots,
                cores,
            ]
        ).astype(jnp.int32)

    for step in range(1, 4):
        state = attend_next(flags_of(step), q_all, up[step], down[step], gate, gate, state)
    partial = attend_last(
        flags_of(4), q_all, up_half, down_half, gate[:, :, :OWN], gate[:, :, OWN:], state
    )

    conv = project(conv_weights)
    width = outer_gate.shape[1]
    gate_outer, gate_inner, conv_input = (conv[:, i * width : (i + 1) * width] for i in range(3))
    mixed_in = (gate_inner.astype(F32) * conv_input.astype(F32)).astype(BF)
    order = ("z", "y", "c")
    count = NZ * NY * NC
    carried = lax.ppermute(mixed_in[OWN - (KTAP - 1) :], order, [(i, i + 1) for i in range(count - 1)])
    padded = jnp.concatenate([carried, mixed_in], axis=0).astype(F32)
    summed = jnp.zeros(mixed_in.shape, F32)
    for offset in range(KTAP):
        summed = summed + conv_taps[offset].astype(F32) * padded[offset : offset + OWN]
    grouped = group_norm(gate_outer.astype(F32) * summed, channel_gain).reshape(NX, ROWS, width)
    gain_rows = jnp.broadcast_to(head_gain[None], (STAT, width))

    def rows_for(place):
        block = lax.dynamic_index_in_dim(grouped, place % NX, 0, keepdims=False)
        return jnp.concatenate([block, gain_rows], axis=0)

    groups = jnp.stack(
        [
            rows_for(x),
            shifted(rows_for(x + 1), "x", 1),
            shifted(rows_for(x + NX - 1), "x", -1),
            shifted(rows_for(x + 2), "x", 2),
        ]
    )
    group_rows, gains = groups[:, :ROWS], groups[:, ROWS:]

    chosen = jnp.where(c == 0, attention_out, channel_out)
    w_left = shifted(chosen, "x", 1)
    w_right = shifted(chosen, "x", -1)
    cut = width // 2
    w_far = (shifted(w_left[:cut], "x", 1), shifted(w_right[cut:], "x", -1))
    first_w = [chosen, w_left, w_right, *w_far]
    second_w = [jnp.where(c == 0, channel_out, attention_out)] + [shifted(w, "c", 1) for w in first_w[1:]]

    parts = partial.reshape(NY * NC * NX, ROWS + STAT, HEAD)
    parts = lax.all_to_all(parts, ("y", "c", "x"), 0, 0, tiled=True)
    where = jnp.stack([x, (x + NX - 1) % NX, (x + 1) % NX, (x + 2) % NX]).astype(jnp.int32)
    heads = merge(where, parts.reshape(NY, NC, NX, ROWS + STAT, HEAD), gains)

    first = jnp.where(c == 0, heads, group_rows)
    second = jnp.where(c == 0, group_rows, heads)
    total = jnp.zeros((ROWS, attention_out.shape[1]), F32)
    for acts, ws in ((first, first_w), (second, second_w)):
        for n in range(3):
            total = total + dot(acts[n], ws[n])
        total = total + dot(acts[3, :, :cut], ws[3]) + dot(acts[3, :, cut:], ws[4])
    return total.astype(BF)


def solution(mesh):
    physical = Mesh(mesh.devices.reshape(NZ, NY, NC, NX), ("z", "y", "c", "x"))
    rows = P(("z", "y", "c", "x"), None)
    cols = P(None, "x")
    placed = (rows,) + (cols,) * 7 + (P("x", None), P("x"), P("x"), P("x", None), P("x", None))
    return jax.shard_map(local, mesh=physical, in_specs=placed, out_specs=rows, check_vma=False)
```

time: 305 us -> 237 us (0.78)
  Pallas kernels: 0 us -> 97.6 us
  waiting for transfers between devices: 111 us -> 26.4 us
  starting transfers between devices: 9.58 us -> 43.3 us
  matrix products: 58 us -> 25.5 us
  local copies, waits for them, and re-layouts: 56.7 us -> 29.4 us
  blocking collectives: 24.8 us -> 0 us
  other arithmetic: 27.7 us -> 10.8 us
  between operations: 13.7 us -> 0.86 us
    all_gather x2 -> x0, waiting for transfers between devices: 101 us -> none  [sent_together(): lax.all_gather(both, axis, axis=dim, tiled=True)]
    pallas_call x0 -> x6, Pallas kernels: none -> 97.6 us  [the longest x3 65.1 us: attend_next(): pl.pallas_call(next_kernel, grid_spec=pltpu.PrefetchScalarGridSpec(num_sc...]
    dynamic_slice x32 -> x1, local copies, waits for them, and re-layouts: 35.3 us -> 0.28 us  [local(): gate = lax.dynamic_slice_in_dim(gate_sum, c, 1, 0).reshape(NZ, NY, NC, OWN)]
    ppermute x1 -> x28, starting transfers between devices: 1.92 us -> 36.5 us  [the longest x27 34.6 us: shifted(): return lax.ppermute(a, axis, [(i, (i + by) % n) for i in range(n)])]
    dot_general x40 -> x16, matrix products: 58 us -> 25.5 us  [dot(): return jnp.dot(a, b, preferred_element_type=F32)]
    all_to_all x1 -> x0, blocking collectives: 24.8 us -> none  [copy_for_each(): lax.all_to_all(jnp.broadcast_to(shard[None], (peers, *shard.shape)), axis...]
    ppermute x1 -> x28, waiting for transfers between devices: 2.25 us -> 26.4 us  [the longest x27 26.4 us: shifted(): return lax.ppermute(a, axis, [(i, (i + by) % n) for i in range(n)])]
    reduce_sum x18 -> x1, other arithmetic: 15.5 us -> 0.48 us  [group_norm(): jnp.mean(shaped * shaped, axis=-1, keepdims=True) + EPS]
  transfers between devices with their start and end apart: 5 -> 29, of which waited for: 4 -> 8; matrix products, arithmetic and copies ran while one was open for 45% -> 22% of each run, Pallas kernels for 0% -> 42%
where the time goes in v1:
time: 237 us; the launch traced here: 234 us
  Pallas kernels  97.6 us (41%)
  starting transfers between devices  43.3 us (18%)
  local copies, waits for them, and re-layouts  29.4 us (12%)
  waiting for transfers between devices  26.4 us (11%)
  matrix products  25.5 us (11%)
  other arithmetic  10.8 us (5%)
    pallas_call x3, Pallas kernels, attend_next(): pl.pallas_call(next_kernel, grid_spec=pltpu.PrefetchScalarGridSpec(num_sc...  65.1 us
    ppermute x27, starting transfers between devices, shifted(): return lax.ppermute(a, axis, [(i, (i + by) % n) for i in range(n)])  34.6 us
    ppermute x27, waiting for transfers between devices, shifted(): return lax.ppermute(a, axis, [(i, (i + by) % n) for i in range(n)])  26.4 us
    dot_general x16, matrix products, dot(): return jnp.dot(a, b, preferred_element_type=F32)  25.5 us
    pallas_call x1, Pallas kernels, attend_last(): pl.pallas_call(last_kernel, grid_spec=pltpu.PrefetchScalarGridSpec(num_sc...  19.6 us
    unnamed x53, local copies, waits for them, and re-layouts  13 us
    pallas_call x1, Pallas kernels, attend_first(): pl.pallas_call(first_kernel, grid_spec=pltpu.PrefetchScalarGridSpec(num_s...  8.42 us
    all_to_all x1, starting transfers between devices, local(): parts = lax.all_to_all(parts, ('y', 'c', 'x'), 0, 0, tiled=True)  6.8 us
  transfers between devices with their start and end apart: 29, of which 8 were waited for; matrix products, arithmetic and copies ran while one was open for 22% of the time, Pallas kernels for 42%

profile of v1, /device:TPU:248, one launch (start us, length us, event | category | flops | bytes accessed | tf_op | source)
XLA Modules:
  0.0 233.9 jit_solution(7179269569712592131)
XLA Ops:
  1.6 1.7 collective-permute-start.1
  3.3 1.9 dynamic-slice_dynamic-update-slice_fusion.5
  5.3 1.9 dynamic-slice_dynamic-update-slice_fusion.4
  7.2 1.9 dynamic-slice_dynamic-update-slice_fusion.3
  17.0 3.3 %fusion.12 = bf16[4,96,768]{2,1,0:T(8,128)(2,1)} fusion(bf16[4,96,768]{2,1,0:T(8,128)(2,1)} %broadcast.39.clone.1, s32[]{:T(128)S(6)} %select_n.166, bf16[96,2048]{1,0:T(8,128)(2,1)S(1)} %copy-done.9, bf16[2048,768]{1,0:T(8,128)(2,1)} %dynamic-slice_dynamic-update-slice_fusion), kind=kOutput, calls=%fused_computation.21 | convolution fusion | flops 302063616 | bytes 3686404 | tf_op jit(solution)/shard_map/dot_general | solution.py:31
  26.8 2.7 %convolution_convert_fusion.1 = bf16[192,768]{1,0:T(8,128)(2,1)S(1)} fusion(bf16[192,2048]{1,0:T(8,128)(2,1)S(1)} %constant_dynamic-update-slice_fusion, bf16[2048,768]{1,0:T(8,128)(2,1)} %dynamic-slice_dynamic-update-slice_fusion), kind=kOutput, calls=%fused_computation.11 | convolution fusion | flops 604127232 | bytes 4227072 | tf_op jit(solution)/shard_map/dot_general | solution.py:31
  32.5 3.1 %collective-permute-start.3 = (bf16[48,2048]{1,0:T(8,128)(2,1)S(1)}, bf16[48,2048]{1,0:T(8,128)(2,1)S(1)}, u32[]{:S(2)}, u32[]{:S(2)}) collective-permute-start(bf16[48,2048]{1,0:T(8,128)(2,1)S(1)} %slice.155), channel_id=1, source_target_pairs={{0,3},{1,0},{2,1},{3,2},{4,7},{5,4},{6,5},{7,6},{8,11},{9,8},{10,9... | collective-permute-start | bytes 589832 | tf_op jit(solution)/shard_map/ppermute | solution.py:27
  36.9 1.6 collective-permute-done.2
  38.9 3.2 %fusion.8 = bf16[4,96,768]{2,1,0:T(8,128)(2,1)} fusion(bf16[4,96,768]{2,1,0:T(8,128)(2,1)} %fusion.25, s32[]{:T(128)S(6)} %select_n.169, bf16[96,2048]{1,0:T(8,128)(2,1)S(1)} %constant_dynamic-update-slice_fusion.2, bf16[2048,768]{1,0:T(8,128)(2,1)} %dynamic-slice_dynamic-update-slice_fusion), kind=kOutput, calls=%fused_computation.17 | convolution fusion | flops 302063616 | bytes 3686404 | tf_op jit(solution)/shard_map/dot_general | solution.py:31
  46.7 2.2 collective-permute-start.8
  51.5 1.9 collective-permute-start.16
  55.9 2.6 %collective-permute-done.12.kvb_ref = bf16[768,256]{1,0:T(8,128)(2,1)} collective-permute-done((bf16[768,256]{1,0:T(8,128)(2,1)}, bf16[768,256]{1,0:T(8,128)(2,1)}, u32[]{:S(2)}, u32[]{:S(2)}) %collective-permute-start.12) | collective-permute-done | bytes 393248 | tf_op jit(solution)/shard_map/ppermute | solution.py:27
  58.5 3.2 %collective-permute-start.9 = (bf16[768,256]{1,0:T(8,128)(2,1)}, bf16[768,256]{1,0:T(8,128)(2,1)}, u32[]{:S(2)}, u32[]{:S(2)}) collective-permute-start(bf16[768,256]{1,0:T(8,128)(2,1)} %collective-permute-done.8.kva_ref), channel_id=1, source_target_pairs={{0,32},{32,64},{64,96},{96,128},{128,160},{160,192},{192,224},{224... | collective-permute-start | bytes 1179656 | tf_op jit(solution)/shard_map/ppermute | solution.py:27
  63.2 1.8 collective-permute-start.6
  68.1 2.7 %collective-permute-done.5 = bf16[768,128]{1,0:T(8,128)(2,1)S(1)} collective-permute-done((bf16[768,128]{1,0:T(8,128)(2,1)S(1)}, bf16[768,128]{1,0:T(8,128)(2,1)S(1)}, u32[]{:S(2)}, u32[]{:S(2)}) %collective-permute-start.5) | collective-permute-done | bytes 196640 | tf_op jit(solution)/shard_map/ppermute | solution.py:27
  71.8 2.5 %collective-permute-done.6 = bf16[768,128]{1,0:T(8,128)(2,1)} collective-permute-done((bf16[768,128]{1,0:T(8,128)(2,1)S(1)}, bf16[768,128]{1,0:T(8,128)(2,1)}, u32[]{:S(2)}, u32[]{:S(2)}) %collective-permute-start.6) | collective-permute-done | bytes 196640 | tf_op jit(solution)/shard_map/ppermute | solution.py:27
  74.3 3.7 %collective-permute-start.21 = (bf16[256,2048]{1,0:T(8,128)(2,1)S(1)}, bf16[256,2048]{1,0:T(8,128)(2,1)}, u32[]{:S(2)}, u32[]{:S(2)}) collective-permute-start(bf16[256,2048]{1,0:T(8,128)(2,1)S(1)} %copy-done.5), channel_id=1, source_target_pairs={{0,3},{1,0},{2,1},{3,2},{4,7},{5,4},{6,5},{7,6},{8,11},{9,8},{10,9... | collective-permute-start | bytes 3145736 | tf_op jit(solution)/shard_map/ppermute | solution.py:27
  78.3 1.7 collective-permute-start.14
  80.0 2.0 pad_maximum_fusion.q_ref
  82.1 8.4 %attend_first.1 = (f32[3072,128]{1,0:T(8,128)}, f32[3072,128]{1,0:T(8,128)}, f32[3072,128]{1,0:T(8,128)}) custom-call(s32[6]{0:T(128)} %pad_add_fusion.1.code_ref, bf16[3072,128]{1,0:T(8,128)(2,1)} %pad_maximum_fusion.q_ref, bf16[768,256]{1,0:T(8,128)(2,1)} %pad_maximum_fusion.1.kv_ref, f32[8,1,768]{2,1,0:T(1,128)} %copy-done.8), custom_call_target="tpu_custom_call" | custom-call | flops 1207959552 | bytes 10223616 | tf_op jit(solution)/shard_map/attend_first/pallas_call | solution.py:162
  90.5 21.7 %attend_next.3 = (f32[3072,128]{1,0:T(8,128)}, f32[3072,128]{1,0:T(8,128)}, f32[3072,128]{1,0:T(8,128)}) custom-call(s32[10]{0:T(128)} %concatenate.77.flag_ref, bf16[3072,128]{1,0:T(8,128)(2,1)} %pad_maximum_fusion.q_ref, bf16[768,256]{1,0:T(8,128)(2,1)} %collective-permute-done.8.kva_ref, ...), custom_call_target="tpu_custom_call", output_to_operand_aliasing={{0}: (6, {}), {1}: (7, {}), {2}: (8, {})} | custom-call | flops 1207959552 | bytes 10223616 | tf_op jit(solution)/shard_map/attend_next/pallas_call | solution.py:177
  112.4 2.3 collective-permute-start.15
  114.7 21.7 %attend_next.4 = (f32[3072,128]{1,0:T(8,128)}, f32[3072,128]{1,0:T(8,128)}, f32[3072,128]{1,0:T(8,128)}) custom-call(s32[10]{0:T(128)} %concatenate.76.flag_ref, bf16[3072,128]{1,0:T(8,128)(2,1)} %pad_maximum_fusion.q_ref, bf16[768,256]{1,0:T(8,128)(2,1)} %collective-permute-done.9.kva_ref, ...), custom_call_target="tpu_custom_call", output_to_operand_aliasing={{0}: (6, {}), {1}: (7, {}), {2}: (8, {})} | custom-call | flops 1207959552 | bytes 10223616 | tf_op jit(solution)/shard_map/attend_next/pallas_call | solution.py:177
  136.4 21.7 %attend_next.5 = (f32[3072,128]{1,0:T(8,128)}, f32[3072,128]{1,0:T(8,128)}, f32[3072,128]{1,0:T(8,128)}) custom-call(s32[10]{0:T(128)} %concatenate.75.flag_ref, bf16[3072,128]{1,0:T(8,128)(2,1)} %pad_maximum_fusion.q_ref, bf16[768,256]{1,0:T(8,128)(2,1)} %copy-done.14, ...), custom_call_target="tpu_custom_call", output_to_operand_aliasing={{0}: (6, {}), {1}: (7, {}), {2}: (8, {})} | custom-call | flops 1207959552 | bytes 10223616 | tf_op jit(solution)/shard_map/attend_next/pallas_call | solution.py:177
  158.8 19.6 %attend_last.1 = bf16[4,2,4,112,128]{4,3,2,1,0:T(8,128)(2,1)} custom-call(s32[10]{0:T(128)} %concatenate.66.flag_ref, bf16[3072,128]{1,0:T(8,128)(2,1)} %pad_maximum_fusion.q_ref, bf16[384,256]{1,0:T(8,128)(2,1)} %copy-done.17, bf16[384,256]{1,0:T(8,128)(2,1)} %copy-done.18, f32[8,1,384]{2,1,0:T(1,128)} %get-tuple-element.42.ga_ref, ...), custom_call_target="tpu_custom_call" | custom-call | flops 1207959552 | bytes 10223616 | tf_op jit(solution)/shard_map/attend_last/pallas_call | solution.py:198
  178.4 6.8 %all-to-all-start = ((bf16[32,112,128]{2,1,0:T(8,128)(2,1)}), bf16[32,112,128]{2,1,0:T(8,128)(2,1)S(1)}, u32[]{:S(2)}, u32[]{:S(2)}) async-start(bf16[32,112,128]{2,1,0:T(8,128)(2,1)} %bitcast.146), calls=%async_computation | async-start | bytes 1835008 | tf_op jit(solution)/shard_map/all_to_all | solution.py:368
  186.4 2.8 %collective-permute-start.23 = (bf16[128,2048]{1,0:T(8,128)(2,1)S(1)}, bf16[128,2048]{1,0:T(8,128)(2,1)}, u32[]{:S(2)}, u32[]{:S(2)}) collective-permute-start(bf16[128,2048]{1,0:T(8,128)(2,1)S(1)} %slice.177), channel_id=1, source_target_pairs={{0,3},{1,0},{2,1},{3,2},{4,7},{5,4},{6,5},{7,6},{8,11},{9,8},{10,9... | collective-permute-start | bytes 1572872 | tf_op jit(solution)/shard_map/ppermute | solution.py:27
  191.8 2.5 %collective-permute-start.18 = (bf16[112,256]{1,0:T(8,128)(2,1)S(1)}, bf16[112,256]{1,0:T(8,128)(2,1)S(1)}, u32[]{:S(2)}, u32[]{:S(2)}) collective-permute-start(bf16[112,256]{1,0:T(8,128)(2,1)S(1)} %get-tuple-element.45), channel_id=1, source_target_pairs={{0,3},{1,0},{2,1},{3,2},{4,7},{5,4},{6,5},{7,6},{8,11},{9,8},{10,9... | collective-permute-start | bytes 172040 | tf_op jit(solution)/shard_map/ppermute | solution.py:27
  196.4 15.2 %collective-permute-done.17 = bf16[112,256]{1,0:T(8,128)(2,1)S(1)} collective-permute-done((bf16[112,256]{1,0:T(8,128)(2,1)S(1)}, bf16[112,256]{1,0:T(8,128)(2,1)S(1)}, u32[]{:S(2)}, u32[]{:S(2)}) %collective-permute-start.17) | collective-permute-done | bytes 57376 | tf_op jit(solution)/shard_map/ppermute | solution.py:27
  215.4 4.5 %merge.1 = bf16[4,96,256]{2,1,0:T(8,128)(2,1)} custom-call(s32[4]{0:T(128)} %pad_add_fusion.where_ref, bf16[4,2,4,112,128]{4,3,2,1,0:T(8,128)(2,1)} %bitcast.145, bf16[4,16,256]{2,1,0:T(8,128)(2,1)} %pad_maximum_fusion.10.gain_ref), custom_call_target="tpu_custom_call" | custom-call | tf_op jit(solution)/shard_map/merge/pallas_call | solution.py:235
  225.1 1.7 fusion.28
  231.6 2.3 fusion.6
  (149 shorter events, 56.1 us)
Async XLA Ops:
  0.0 24.7 %collective-permute-start = (bf16[96,2048]{1,0:T(8,128)(2,1)}, bf16[96,2048]{1,0:T(8,128)(2,1)}, u32[]{:S(2)}, u32[]{:S(2)}) collective-permute-start(bf16[96,2048]{1,0:T(8,128)(2,1)} %param.13), channel_id=1, source_target_pairs={{0,1},{1,2},{2,3},{3,0},{4,5},{5,6},{6,7},{7,4},{8,9},{9,10},{10,1... | collective-permute-start | bytes 1179656 | tf_op jit(solution)/shard_map/ppermute | solution.py:27
  1.6 24.1 %collective-permute-start.1 = (bf16[96,2048]{1,0:T(8,128)(2,1)}, bf16[96,2048]{1,0:T(8,128)(2,1)}, u32[]{:S(2)}, u32[]{:S(2)}) collective-permute-start(bf16[96,2048]{1,0:T(8,128)(2,1)} %param.13), channel_id=1, source_target_pairs={{0,3},{1,0},{2,1},{3,2},{4,7},{5,4},{6,5},{7,6},{8,11},{9,8},{10,9... | collective-permute-start | bytes 1179656 | tf_op jit(solution)/shard_map/ppermute | solution.py:27
  31.2 7.4 %collective-permute-start.2 = (bf16[48,2048]{1,0:T(8,128)(2,1)S(1)}, bf16[48,2048]{1,0:T(8,128)(2,1)S(1)}, u32[]{:S(2)}, u32[]{:S(2)}) collective-permute-start(bf16[48,2048]{1,0:T(8,128)(2,1)S(1)} %slice.154), channel_id=1, source_target_pairs={{0,1},{1,2},{2,3},{3,0},{4,5},{5,6},{6,7},{7,4},{8,9},{9,10},{10,1... | collective-permute-start | bytes 589832 | tf_op jit(solution)/shard_map/ppermute | solution.py:27
  32.5 6.4 %collective-permute-start.3 = (bf16[48,2048]{1,0:T(8,128)(2,1)S(1)}, bf16[48,2048]{1,0:T(8,128)(2,1)S(1)}, u32[]{:S(2)}, u32[]{:S(2)}) collective-permute-start(bf16[48,2048]{1,0:T(8,128)(2,1)S(1)} %slice.155), channel_id=1, source_target_pairs={{0,3},{1,0},{2,1},{3,2},{4,7},{5,4},{6,5},{7,6},{8,11},{9,8},{10,9... | collective-permute-start | bytes 589832 | tf_op jit(solution)/shard_map/ppermute | solution.py:27
  43.2 1.7 collective-permute-start.4
  45.7 12.8 %collective-permute-start.12 = (bf16[768,256]{1,0:T(8,128)(2,1)}, bf16[768,256]{1,0:T(8,128)(2,1)}, u32[]{:S(2)}, u32[]{:S(2)}) collective-permute-start(bf16[768,256]{1,0:T(8,128)(2,1)} %pad_maximum_fusion.1.kv_ref), channel_id=1, source_target_pairs={{0,224},{32,0},{64,32},{96,64},{128,96},{160,128},{192,160},{224,1... | collective-permute-start | bytes 1179656 | tf_op jit(solution)/shard_map/ppermute | solution.py:27
  46.7 11.8 %collective-permute-start.8 = (bf16[768,256]{1,0:T(8,128)(2,1)}, bf16[768,256]{1,0:T(8,128)(2,1)}, u32[]{:S(2)}, u32[]{:S(2)}) collective-permute-start(bf16[768,256]{1,0:T(8,128)(2,1)} %pad_maximum_fusion.1.kv_ref), channel_id=1, source_target_pairs={{0,32},{32,64},{64,96},{96,128},{128,160},{160,192},{192,224},{224... | collective-permute-start | bytes 1179656 | tf_op jit(solution)/shard_map/ppermute | solution.py:27
  51.5 10.3 %collective-permute-start.16 = (bf16[2,256]{1,0:T(2,128)(2,1)S(1)}, bf16[2,256]{1,0:T(2,128)(2,1)S(1)}, u32[]{:S(2)}, u32[]{:S(2)}) collective-permute-start(bf16[2,256]{1,0:T(2,128)(2,1)S(1)} %slice.167), channel_id=1, source_target_pairs={{0,4},{4,8},{8,12},{12,16},{16,20},{20,24},{24,28},{28,32},{32,36}... | collective-permute-start | bytes 3080 | tf_op jit(solution)/shard_map/ppermute | solution.py:337
  58.5 19.8 %collective-permute-start.13 = (bf16[768,256]{1,0:T(8,128)(2,1)}, bf16[768,256]{1,0:T(8,128)(2,1)S(1)}, u32[]{:S(2)}, u32[]{:S(2)}) collective-permute-start(bf16[768,256]{1,0:T(8,128)(2,1)} %collective-permute-done.12.kvb_ref), channel_id=1, source_target_pairs={{0,224},{32,0},{64,32},{96,64},{128,96},{160,128},{192,160},{224,1... | collective-permute-start | bytes 1179656 | tf_op jit(solution)/shard_map/ppermute | solution.py:27
  58.5 19.5 %collective-permute-start.9 = (bf16[768,256]{1,0:T(8,128)(2,1)}, bf16[768,256]{1,0:T(8,128)(2,1)}, u32[]{:S(2)}, u32[]{:S(2)}) collective-permute-start(bf16[768,256]{1,0:T(8,128)(2,1)} %collective-permute-done.8.kva_ref), channel_id=1, source_target_pairs={{0,32},{32,64},{64,96},{96,128},{128,160},{160,192},{192,224},{224... | collective-permute-start | bytes 1179656 | tf_op jit(solution)/shard_map/ppermute | solution.py:27
  62.8 8.0 %collective-permute-start.5 = (bf16[768,128]{1,0:T(8,128)(2,1)S(1)}, bf16[768,128]{1,0:T(8,128)(2,1)S(1)}, u32[]{:S(2)}, u32[]{:S(2)}) collective-permute-start(bf16[768,128]{1,0:T(8,128)(2,1)S(1)} %pad_maximum_fusion.5), channel_id=1, source_target_pairs={{0,8},{8,16},{16,24},{24,0},{1,9},{9,17},{17,25},{25,1},{2,10},{10... | collective-permute-start | bytes 589832 | tf_op jit(solution)/shard_map/ppermute | solution.py:27
  63.2 11.0 %collective-permute-start.6 = (bf16[768,128]{1,0:T(8,128)(2,1)S(1)}, bf16[768,128]{1,0:T(8,128)(2,1)}, u32[]{:S(2)}, u32[]{:S(2)}) collective-permute-start(bf16[768,128]{1,0:T(8,128)(2,1)S(1)} %pad_maximum_fusion.5), channel_id=1, source_target_pairs={{0,24},{8,0},{16,8},{24,16},{1,25},{9,1},{17,9},{25,17},{2,26},{10... | collective-permute-start | bytes 589832 | tf_op jit(solution)/shard_map/ppermute | solution.py:27
  65.0 15.0 %collective-permute-start.7 = (bf16[768,128]{1,0:T(8,128)(2,1)S(1)}, bf16[768,128]{1,0:T(8,128)(2,1)}, u32[]{:S(2)}, u32[]{:S(2)}) collective-permute-start(bf16[768,128]{1,0:T(8,128)(2,1)S(1)} %pad_maximum_fusion.5), channel_id=1, source_target_pairs={{0,16},{8,24},{16,0},{24,8},{1,17},{9,25},{17,1},{25,9},{2,18},{10... | collective-permute-start | bytes 589832 | tf_op jit(solution)/shard_map/ppermute | solution.py:27
  70.8 118.4 %collective-permute-start.20 = (bf16[256,2048]{1,0:T(8,128)(2,1)S(1)}, bf16[256,2048]{1,0:T(8,128)(2,1)}, u32[]{:S(2)}, u32[]{:S(2)}) collective-permute-start(bf16[256,2048]{1,0:T(8,128)(2,1)S(1)} %copy-done.5), channel_id=1, source_target_pairs={{0,1},{1,2},{2,3},{3,0},{4,5},{5,6},{6,7},{7,4},{8,9},{9,10},{10,1... | collective-permute-start | bytes 3145736 | tf_op jit(solution)/shard_map/ppermute | solution.py:27
  74.3 111.0 %collective-permute-start.21 = (bf16[256,2048]{1,0:T(8,128)(2,1)S(1)}, bf16[256,2048]{1,0:T(8,128)(2,1)}, u32[]{:S(2)}, u32[]{:S(2)}) collective-permute-start(bf16[256,2048]{1,0:T(8,128)(2,1)S(1)} %copy-done.5), channel_id=1, source_target_pairs={{0,3},{1,0},{2,1},{3,2},{4,7},{5,4},{6,5},{7,6},{8,11},{9,8},{10,9... | collective-permute-start | bytes 3145736 | tf_op jit(solution)/shard_map/ppermute | solution.py:27
  78.0 34.2 %collective-permute-start.10 = (bf16[768,256]{1,0:T(8,128)(2,1)}, bf16[768,256]{1,0:T(8,128)(2,1)S(1)}, u32[]{:S(2)}, u32[]{:S(2)}) collective-permute-start(bf16[768,256]{1,0:T(8,128)(2,1)} %collective-permute-done.9.kva_ref), channel_id=1, source_target_pairs={{0,32},{32,64},{64,96},{96,128},{128,160},{160,192},{192,224},{224... | collective-permute-start | bytes 1179656 | tf_op jit(solution)/shard_map/ppermute | solution.py:27
  78.3 33.9 %copy-start.16 = (bf16[768,256]{1,0:T(8,128)(2,1)}, bf16[768,256]{1,0:T(8,128)(2,1)S(1)}, u32[]{:S(2)}) copy-start(bf16[768,256]{1,0:T(8,128)(2,1)S(1)} %collective-permute-done.13.kvb_ref) | copy-start | bytes 1179652
  78.3 34.0 %collective-permute-start.14 = (bf16[768,256]{1,0:T(8,128)(2,1)S(1)}, bf16[768,256]{1,0:T(8,128)(2,1)S(1)}, u32[]{:S(2)}, u32[]{:S(2)}) collective-permute-start(bf16[768,256]{1,0:T(8,128)(2,1)S(1)} %collective-permute-done.13.kvb_ref), channel_id=1, source_target_pairs={{0,224},{32,0},{64,32},{96,64},{128,96},{160,128},{192,160},{224,1... | collective-permute-start | bytes 1179656 | tf_op jit(solution)/shard_map/ppermute | solution.py:27
  112.2 24.2 %copy-start.14 = (bf16[768,256]{1,0:T(8,128)(2,1)}, bf16[768,256]{1,0:T(8,128)(2,1)S(1)}, u32[]{:S(2)}) copy-start(bf16[768,256]{1,0:T(8,128)(2,1)S(1)} %collective-permute-done.10.kva_ref) | copy-start | bytes 1179652
  112.3 45.9 %collective-permute-start.11 = (bf16[384,256]{1,0:T(8,128)(2,1)S(1)}, bf16[384,256]{1,0:T(8,128)(2,1)S(1)}, u32[]{:S(2)}, u32[]{:S(2)}) collective-permute-start(bf16[384,256]{1,0:T(8,128)(2,1)S(1)} %slice.158), channel_id=1, source_target_pairs={{0,32},{32,64},{64,96},{96,128},{128,160},{160,192},{192,224},{224... | collective-permute-start | bytes 589832 | tf_op jit(solution)/shard_map/ppermute | solution.py:27
  112.4 24.0 %copy-start.15 = (bf16[768,256]{1,0:T(8,128)(2,1)}, bf16[768,256]{1,0:T(8,128)(2,1)S(1)}, u32[]{:S(2)}) copy-start(bf16[768,256]{1,0:T(8,128)(2,1)S(1)} %collective-permute-done.14.kvb_ref) | copy-start | bytes 1179652
  112.4 45.7 %collective-permute-start.15 = (bf16[384,256]{1,0:T(8,128)(2,1)S(1)}, bf16[384,256]{1,0:T(8,128)(2,1)S(1)}, u32[]{:S(2)}, u32[]{:S(2)}) collective-permute-start(bf16[384,256]{1,0:T(8,128)(2,1)S(1)} %slice.159), channel_id=1, source_target_pairs={{0,224},{32,0},{64,32},{96,64},{128,96},{160,128},{192,160},{224,1... | collective-permute-start | bytes 589832 | tf_op jit(solution)/shard_map/ppermute | solution.py:27
  178.4 36.0 %all-to-all-start = ((bf16[32,112,128]{2,1,0:T(8,128)(2,1)}), bf16[32,112,128]{2,1,0:T(8,128)(2,1)S(1)}, u32[]{:S(2)}, u32[]{:S(2)}) async-start(bf16[32,112,128]{2,1,0:T(8,128)(2,1)} %bitcast.146), calls=%async_computation | async-start | bytes 1835008 | tf_op jit(solution)/shard_map/all_to_all | solution.py:368
  186.4 27.6 %collective-permute-start.23 = (bf16[128,2048]{1,0:T(8,128)(2,1)S(1)}, bf16[128,2048]{1,0:T(8,128)(2,1)}, u32[]{:S(2)}, u32[]{:S(2)}) collective-permute-start(bf16[128,2048]{1,0:T(8,128)(2,1)S(1)} %slice.177), channel_id=1, source_target_pairs={{0,3},{1,0},{2,1},{3,2},{4,7},{5,4},{6,5},{7,6},{8,11},{9,8},{10,9... | collective-permute-start | bytes 1572872 | tf_op jit(solution)/shard_map/ppermute | solution.py:27
  190.3 23.7 %collective-permute-start.22 = (bf16[128,2048]{1,0:T(8,128)(2,1)S(1)}, bf16[128,2048]{1,0:T(8,128)(2,1)}, u32[]{:S(2)}, u32[]{:S(2)}) collective-permute-start(bf16[128,2048]{1,0:T(8,128)(2,1)S(1)} %slice.175), channel_id=1, source_target_pairs={{0,1},{1,2},{2,3},{3,0},{4,5},{5,6},{6,7},{7,4},{8,9},{9,10},{10,1... | collective-permute-start | bytes 1572872 | tf_op jit(solution)/shard_map/ppermute | solution.py:27
  191.0 20.6 %collective-permute-start.17 = (bf16[112,256]{1,0:T(8,128)(2,1)S(1)}, bf16[112,256]{1,0:T(8,128)(2,1)S(1)}, u32[]{:S(2)}, u32[]{:S(2)}) collective-permute-start(bf16[112,256]{1,0:T(8,128)(2,1)S(1)} %get-tuple-element.44), channel_id=1, source_target_pairs={{0,1},{1,2},{2,3},{3,0},{4,5},{5,6},{6,7},{7,4},{8,9},{9,10},{10,1... | collective-permute-start | bytes 172040 | tf_op jit(solution)/shard_map/ppermute | solution.py:27
  191.8 19.8 %collective-permute-start.18 = (bf16[112,256]{1,0:T(8,128)(2,1)S(1)}, bf16[112,256]{1,0:T(8,128)(2,1)S(1)}, u32[]{:S(2)}, u32[]{:S(2)}) collective-permute-start(bf16[112,256]{1,0:T(8,128)(2,1)S(1)} %get-tuple-element.45), channel_id=1, source_target_pairs={{0,3},{1,0},{2,1},{3,2},{4,7},{5,4},{6,5},{7,6},{8,11},{9,8},{10,9... | collective-permute-start | bytes 172040 | tf_op jit(solution)/shard_map/ppermute | solution.py:27
  194.3 18.5 %collective-permute-start.19 = (bf16[112,256]{1,0:T(8,128)(2,1)S(1)}, bf16[112,256]{1,0:T(8,128)(2,1)S(1)}, u32[]{:S(2)}, u32[]{:S(2)}) collective-permute-start(bf16[112,256]{1,0:T(8,128)(2,1)S(1)} %get-tuple-element.46), channel_id=1, source_target_pairs={{0,2},{1,3},{2,0},{3,1},{4,6},{5,7},{6,4},{7,5},{8,10},{9,11},{10,... | collective-permute-start | bytes 172040 | tf_op jit(solution)/shard_map/ppermute | solution.py:27
  213.4 11.7 %collective-permute-start.25 = (bf16[256,2048]{1,0:T(8,128)(2,1)}, bf16[256,2048]{1,0:T(8,128)(2,1)}, u32[]{:S(2)}, u32[]{:S(2)}) collective-permute-start(bf16[256,2048]{1,0:T(8,128)(2,1)} %collective-permute-done.21), channel_id=1, source_target_pairs={{0,4},{4,0},{1,5},{5,1},{2,6},{6,2},{3,7},{7,3},{8,12},{12,8},{9,1... | collective-permute-start | bytes 3145736 | tf_op jit(solution)/shard_map/ppermute | solution.py:27
  213.4 18.1 %collective-permute-start.24 = (bf16[256,2048]{1,0:T(8,128)(2,1)}, bf16[256,2048]{1,0:T(8,128)(2,1)}, u32[]{:S(2)}, u32[]{:S(2)}) collective-permute-start(bf16[256,2048]{1,0:T(8,128)(2,1)} %collective-permute-done.20), channel_id=1, source_target_pairs={{0,4},{4,0},{1,5},{5,1},{2,6},{6,2},{3,7},{7,3},{8,12},{12,8},{9,1... | collective-permute-start | bytes 3145736 | tf_op jit(solution)/shard_map/ppermute | solution.py:27
  214.0 9.8 %collective-permute-start.26 = (bf16[128,2048]{1,0:T(8,128)(2,1)}, bf16[128,2048]{1,0:T(8,128)(2,1)}, u32[]{:S(2)}, u32[]{:S(2)}) collective-permute-start(bf16[128,2048]{1,0:T(8,128)(2,1)} %collective-permute-done.22), channel_id=1, source_target_pairs={{0,4},{4,0},{1,5},{5,1},{2,6},{6,2},{3,7},{7,3},{8,12},{12,8},{9,1... | collective-permute-start | bytes 1572872 | tf_op jit(solution)/shard_map/ppermute | solution.py:27
  214.0 12.8 %collective-permute-start.27 = (bf16[128,2048]{1,0:T(8,128)(2,1)}, bf16[128,2048]{1,0:T(8,128)(2,1)}, u32[]{:S(2)}, u32[]{:S(2)}) collective-permute-start(bf16[128,2048]{1,0:T(8,128)(2,1)} %collective-permute-done.23), channel_id=1, source_target_pairs={{0,4},{4,0},{1,5},{5,1},{2,6},{6,2},{3,7},{7,3},{8,12},{12,8},{9,1... | collective-permute-start | bytes 1572872 | tf_op jit(solution)/shard_map/ppermute | solution.py:27
  (19 other events, 117.9 us)
